TPU v7x, 32 devices: a whole 2x2x4 slice. The times are simulated.
32 devices in a mesh: grp: 2 (over y), fs: 4 (over z), tp: 4 (over x, core).
Axes of the slice: x: 2, y: 2, z: 4, core: 2. Of those that a mesh axis runs over, the one named last changes fastest.
Arguments:
- tokens: bfloat16 [2048, 2048], P(('grp', 'fs')), parts along dimension 0, may hold values from -6 to 6
- route_ids: int32 [2048, 2], P(('grp', 'fs')), parts along dimension 0, may hold values from 0 to 7, as said below
- route_weights: float32 [2048, 2], P(('grp', 'fs')), parts along dimension 0, may hold values from 0.2 to 1
- ffn_gain: float32 [2048], P('fs'), may hold values from 0.1 to 1.9
- gate_master: float32 [8, 2048, 1024], P(None, 'fs', 'tp'), may hold values from -0.125 to 0.125
- up_master: float32 [8, 2048, 1024], P(None, 'fs', 'tp'), may hold values from -0.125 to 0.125
- down_master: float32 [8, 1024, 2048], P(None, 'fs', 'tp'), may hold values from -0.1875 to 0.1875
Outputs:
- gate_serve: bfloat16 [16, 2048, 1024], P(('grp', 'fs'), None, 'tp'), parts along dimension 0
- up_serve: bfloat16 [16, 2048, 1024], P(('grp', 'fs'), None, 'tp'), parts along dimension 0
- down_serve: bfloat16 [16, 1024, 2048], P(('grp', 'fs'), None, 'tp'), parts along dimension 0
- mixed: bfloat16 [2048, 2048], P(('grp', 'fs'), 'tp'), parts along dimension 0
There are 2 independent parts, one for each index of `grp`. A program takes and returns all parts, laid end to end along the dimension named above; an argument that names none is the same for every part. Nothing has to cross between parts.
Inputs may be any that keep to these rules, and one draw needn't show every extreme that they name: `route_ids`: each row names two different experts of one group of 8 consecutive experts. Among the tokens of one index of fs, each group is named by exactly 256 tokens and no expert by more than 128; in every group one expert, the same for every index of fs, is named by exactly 128, and so is one other expert of the group, which may change from one index of fs to the next.
All inputs are finite; a program needn't handle non-finite values.
Results may differ from a plain program's by a relative error of at most 0.0087.
Values may be sent and summed in bfloat16 or wider, within the bound.
A program may use at most 64 MiB of HBM per device.

v0:
```python
import jax
import jax.numpy as jnp
from jax import lax
from jax.sharding import PartitionSpec as P

GROUP_SIZE = 8


def slot_targets(route_ids, experts, capacity):
    flat_ids = route_ids.reshape(-1)
    member = (flat_ids[:, None] == jnp.arange(experts, dtype=jnp.int32)[None, :]).astype(jnp.int32)
    before = jnp.cumsum(member, axis=0) - member
    slot_index = jnp.sum(before * member, axis=1)
    return flat_ids * capacity + slot_index


def fill_slots(source, targets, experts, capacity):
    doubled = jnp.repeat(source, 2, axis=0)
    buffer = jnp.zeros((experts * capacity, source.shape[1]), source.dtype).at[targets].set(doubled)
    return buffer.reshape(experts, capacity, source.shape[1])


def on_device(tokens, route_ids, route_weights, ffn_gain, gate_master, up_master, down_master):
    row_gain = ffn_gain[None, :, None]
    gate_local = (gate_master * row_gain).astype(jnp.bfloat16)
    up_local = (up_master * row_gain).astype(jnp.bfloat16)
    down_local = down_master.astype(jnp.bfloat16)
    gate_serve, up_serve, down_serve = (
        lax.all_to_all(gate_local, "fs", split_axis=0, concat_axis=1, tiled=True),
        lax.all_to_all(up_local, "fs", split_axis=0, concat_axis=1, tiled=True),
        lax.all_to_all(down_local, "fs", split_axis=0, concat_axis=1, tiled=True),
    )
    experts = gate_local.shape[0]
    capacity = tokens.shape[0] // (2 * (experts // GROUP_SIZE))
    token_rows = tokens.astype(jnp.float32)
    normed = (
        token_rows * lax.rsqrt(jnp.mean(token_rows * token_rows, axis=1, keepdims=True) + 1e-06)
    ).astype(jnp.bfloat16)
    targets = slot_targets(route_ids, experts, capacity)
    col_width = normed.shape[1] // lax.axis_size("tp")
    own_cols = lax.dynamic_slice_in_dim(normed, lax.axis_index("tp") * col_width, col_width, 1)
    part_rows = lax.all_to_all(
        fill_slots(own_cols, targets, experts, capacity),
        "fs",
        split_axis=0,
        concat_axis=1,
        tiled=True,
    )
    portion = lax.all_gather(part_rows, "tp", axis=2, tiled=True)
    gate_part = jnp.einsum("erd,edf->erf", portion, gate_serve, preferred_element_type=jnp.float32)
    up_part = jnp.einsum("erd,edf->erf", portion, up_serve, preferred_element_type=jnp.float32)
    hidden = (jax.nn.silu(gate_part) * up_part).astype(jnp.bfloat16)
    expert_out = jnp.einsum(
        "erf,efd->erd",
        lax.all_gather(hidden, "tp", axis=2, tiled=True),
        down_serve,
        preferred_element_type=jnp.float32,
    ).astype(jnp.bfloat16)
    returned_rows = lax.all_to_all(expert_out, "fs", split_axis=1, concat_axis=0, tiled=True)
    picked = returned_rows.reshape(-1, returned_rows.shape[2])[targets].astype(jnp.float32)
    weighted = picked * route_weights.reshape(-1, 1)
    combined = jnp.sum(weighted.reshape(-1, 2, returned_rows.shape[2]), axis=1).astype(jnp.bfloat16)
    return (gate_serve, up_serve, down_serve, combined)


def solution(mesh):
    in_specs = (
        P(("grp", "fs"), None),
        P(("grp", "fs"), None),
        P(("grp", "fs"), None),
        P("fs"),
        P(None, "fs", "tp"),
        P(None, "fs", "tp"),
        P(None, "fs", "tp"),
    )
    out_specs = (
        P(("grp", "fs"), None, "tp"),
        P(("grp", "fs"), None, "tp"),
        P(("grp", "fs"), None, "tp"),
        P(("grp", "fs"), "tp"),
    )
    return jax.shard_map(
        on_device, mesh=mesh, in_specs=in_specs, out_specs=out_specs, check_vma=False
    )
```

profile of v0, /device:TPU:0, one launch (start us, length us, event | category | flops | bytes accessed | tf_op | source)
XLA Modules:
  0.0 250.0 jit_solution(12472034540438758420)
XLA Ops:
  7.2 1.5 convert_element_type.43
  11.9 3.5 %scatter_custom_fusion = bf16[1024,512]{1,0:T(8,128)(2,1)} fusion(s32[512]{0:T(512)S(1)} %bitcast.49, bf16[512,512]{1,0:T(8,128)(2,1)S(1)} %reshape.101, bf16[]{:T(256)} %constant.11.clone.1), kind=kCustom, calls=%fused_computation.11 | custom fusion | bytes 1048578 | tf_op jit(solution)/shard_map/scatter | solution.py:19
  15.4 6.3 %all-to-all-start.3 = ((bf16[8,128,512]{2,1,0:T(8,128)(2,1)}), bf16[8,128,512]{2,1,0:T(8,128)(2,1)S(1)}, u32[]{:S(2)}, u32[]{:S(2)}) async-start(bf16[8,128,512]{2,1,0:T(8,128)(2,1)} %bitcast.13), calls=%async_computation.3 | async-start | bytes 2097152 | tf_op jit(solution)/shard_map/all_to_all | solution.py:42
  21.7 6.5 %multiply_convert_fusion = (bf16[8,512,256]{2,1,0:T(8,128)(2,1)}, bf16[8,512,256]{2,1,0:T(8,128)(2,1)}) fusion(f32[8,512,256]{2,1,0:T(8,128)} %param.12, f32[512]{0:T(512)S(1)} %copy-done.4, f32[8,512,256]{2,1,0:T(8,128)} %param.11), kind=kLoop, calls=%fused_computation.2 | loop fusion | flops 4194304 | bytes 12584960 | tf_op jit(solution)/shard_map/convert_element_type | solution.py:26
  28.2 19.3 %all-to-all-done.3 = bf16[8,128,512]{2,1,0:T(8,128)(2,1)S(1)} async-done(((bf16[8,128,512]{2,1,0:T(8,128)(2,1)}), bf16[8,128,512]{2,1,0:T(8,128)(2,1)S(1)}, u32[]{:S(2)}, u32[]{:S(2)}) %all-to-all-start.3) | async-done | bytes 1048608 | tf_op jit(solution)/shard_map/all_to_all | solution.py:42
  47.5 3.6 %all-to-all-start = ((bf16[8,512,256]{2,1,0:T(8,128)(2,1)}), bf16[8,512,256]{2,1,0:T(8,128)(2,1)S(1)}, u32[]{:S(2)}, u32[]{:S(2)}) async-start(bf16[8,512,256]{2,1,0:T(8,128)(2,1)} %get-tuple-element.5), calls=%async_computation | async-start | bytes 4194304 | tf_op jit(solution)/shard_map/all_to_all | solution.py:29
  51.1 1.2 copy.31
  52.3 46.5 %all-to-all-done = bf16[8,512,256]{2,1,0:T(8,128)(2,1)S(1)} async-done(((bf16[8,512,256]{2,1,0:T(8,128)(2,1)}), bf16[8,512,256]{2,1,0:T(8,128)(2,1)S(1)}, u32[]{:S(2)}, u32[]{:S(2)}) %all-to-all-start) | async-done | bytes 2097184 | tf_op jit(solution)/shard_map/all_to_all | solution.py:29
  98.8 4.5 %all-to-all-start.1 = ((bf16[8,512,256]{2,1,0:T(8,128)(2,1)}), bf16[8,512,256]{2,1,0:T(8,128)(2,1)}, u32[]{:S(2)}, u32[]{:S(2)}) async-start(bf16[8,512,256]{2,1,0:T(8,128)(2,1)} %get-tuple-element.4), calls=%async_computation.1 | async-start | bytes 4194304 | tf_op jit(solution)/shard_map/all_to_all | solution.py:30
  103.3 3.8 %convert_element_type.40 = bf16[8,256,512]{2,1,0:T(8,128)(2,1)} convert(f32[8,256,512]{2,1,0:T(8,128)} %param.13) | non-fusion elementwise | flops 1048576 | bytes 6291456 | tf_op jit(solution)/shard_map/convert_element_type | solution.py:27
  107.0 1.5 copy.25
  108.5 42.6 %all-to-all-done.1 = bf16[8,512,256]{2,1,0:T(8,128)(2,1)} async-done(((bf16[8,512,256]{2,1,0:T(8,128)(2,1)}), bf16[8,512,256]{2,1,0:T(8,128)(2,1)}, u32[]{:S(2)}, u32[]{:S(2)}) %all-to-all-start.1) | async-done | bytes 2097184 | tf_op jit(solution)/shard_map/all_to_all | solution.py:30
  151.1 3.6 %all-to-all-start.2 = ((bf16[8,256,512]{2,1,0:T(8,128)(2,1)}), bf16[8,256,512]{2,1,0:T(8,128)(2,1)S(1)}, u32[]{:S(2)}, u32[]{:S(2)}) async-start(bf16[8,256,512]{2,1,0:T(8,128)(2,1)} %convert_element_type.40), calls=%async_computation.2 | async-start | bytes 4194304 | tf_op jit(solution)/shard_map/all_to_all | solution.py:31
  154.7 3.0 %copy.26 = bf16[4,2,512,256]{3,2,0,1:T(8,128)(2,1)} copy(bf16[4,2,512,256]{3,2,1,0:T(8,128)(2,1)} %bitcast.3) | data formatting | bytes 4194304 | tf_op jit(solution)/shard_map/all_to_all | solution.py:30
  157.8 4.2 %fusion.7 = f32[2,512,256]{2,1,0:T(8,128)S(1)} fusion(bf16[2,512,2048]{2,1,0:T(8,128)(2,1)} %all-gather.3.cloned.1.call-done, bf16[2,2048,256]{2,1,0:T(8,128)(2,1)} %bitcast.43), kind=kOutput, calls=%fused_computation.24 | convolution fusion | flops 1073741824 | bytes 7340032 | tf_op jit(solution)/shard_map/erd,edf->erf/dot_general | solution.py:50
  162.5 2.1 fusion
  164.6 37.8 %all-to-all-done.2 = bf16[8,256,512]{2,1,0:T(8,128)(2,1)S(1)} async-done(((bf16[8,256,512]{2,1,0:T(8,128)(2,1)}), bf16[8,256,512]{2,1,0:T(8,128)(2,1)S(1)}, u32[]{:S(2)}, u32[]{:S(2)}) %all-to-all-start.2) | async-done | bytes 2097184 | tf_op jit(solution)/shard_map/all_to_all | solution.py:31
  202.4 1.5 copy.27
  204.0 3.5 %convolution_convert_fusion = bf16[2,512,512]{2,1,0:T(8,128)(2,1)S(1)} fusion(bf16[2,512,1024]{2,1,0:T(8,128)(2,1)} %all-gather.5.cloned.1.call-done, bf16[2,1024,512]{2,1,0:T(8,128)(2,1)} %bitcast.47), kind=kOutput, calls=%fused_computation.5 | convolution fusion | flops 1074266112 | bytes 5242880 | tf_op jit(solution)/shard_map/erf,efd->erd/dot_general | solution.py:53
  207.4 2.0 copy.32
  209.5 3.7 %all-to-all-start.4 = ((bf16[2,512,512]{2,0,1:T(2,128)(2,1)}), bf16[2,512,512]{2,0,1:T(2,128)(2,1)S(1)}, u32[]{:S(2)}, u32[]{:S(2)}) async-start(bf16[2,512,512]{2,0,1:T(2,128)(2,1)} %copy.32), calls=%async_computation.4 | async-start | bytes 2097152 | tf_op jit(solution)/shard_map/all_to_all | solution.py:59
  213.4 24.9 %all-to-all-done.4 = bf16[2,512,512]{2,0,1:T(2,128)(2,1)S(1)} async-done(((bf16[2,512,512]{2,0,1:T(2,128)(2,1)}), bf16[2,512,512]{2,0,1:T(2,128)(2,1)S(1)}, u32[]{:S(2)}, u32[]{:S(2)}) %all-to-all-start.4) | async-done | bytes 1048608 | tf_op jit(solution)/shard_map/all_to_all | solution.py:59
  238.4 2.0 gather_fusion
  241.1 2.1 multiply_reduce_fusion.1
  (40 shorter events, 4.6 us)
Async XLA Ops:
  7.2 1.6 copy-start
  7.2 1.9 copy-start.2
  9.9 11.8 %copy-start.4 = (f32[512]{0:T(512)S(1)}, f32[512]{0:T(512)}, u32[]{:S(2)}) copy-start(f32[512]{0:T(512)} %param.10) | copy-start | bytes 6148
  15.4 32.1 %all-to-all-start.3 = ((bf16[8,128,512]{2,1,0:T(8,128)(2,1)}), bf16[8,128,512]{2,1,0:T(8,128)(2,1)S(1)}, u32[]{:S(2)}, u32[]{:S(2)}) async-start(bf16[8,128,512]{2,1,0:T(8,128)(2,1)} %bitcast.13), calls=%async_computation.3 | async-start | bytes 2097152 | tf_op jit(solution)/shard_map/all_to_all | solution.py:42
  47.5 51.3 %all-to-all-start = ((bf16[8,512,256]{2,1,0:T(8,128)(2,1)}), bf16[8,512,256]{2,1,0:T(8,128)(2,1)S(1)}, u32[]{:S(2)}, u32[]{:S(2)}) async-start(bf16[8,512,256]{2,1,0:T(8,128)(2,1)} %get-tuple-element.5), calls=%async_computation | async-start | bytes 4194304 | tf_op jit(solution)/shard_map/all_to_all | solution.py:29
  51.1 106.7 %all-gather.3.cloned.1.call-start = ((), (), s32[]{:S(2)}) async-start(), calls=%async_computation.5 | async-start | bytes 5242880 | tf_op jit(solution)/shard_map/all_gather | solution.py:49
  98.8 52.3 %all-to-all-start.1 = ((bf16[8,512,256]{2,1,0:T(8,128)(2,1)}), bf16[8,512,256]{2,1,0:T(8,128)(2,1)}, u32[]{:S(2)}, u32[]{:S(2)}) async-start(bf16[8,512,256]{2,1,0:T(8,128)(2,1)} %get-tuple-element.4), calls=%async_computation.1 | async-start | bytes 4194304 | tf_op jit(solution)/shard_map/all_to_all | solution.py:30
  151.1 51.3 %all-to-all-start.2 = ((bf16[8,256,512]{2,1,0:T(8,128)(2,1)}), bf16[8,256,512]{2,1,0:T(8,128)(2,1)S(1)}, u32[]{:S(2)}, u32[]{:S(2)}) async-start(bf16[8,256,512]{2,1,0:T(8,128)(2,1)} %convert_element_type.40), calls=%async_computation.2 | async-start | bytes 4194304 | tf_op jit(solution)/shard_map/all_to_all | solution.py:31
  154.7 49.3 %all-gather.5.cloned.1.call-start = ((), (), s32[]{:S(2)}) async-start(), calls=%async_computation.6 | async-start | bytes 2621440 | tf_op jit(solution)/shard_map/all_gather | solution.py:55
  157.8 4.3 %copy-start.1 = (bf16[4,2,512,256]{3,2,0,1:T(8,128)(2,1)S(1)}, bf16[4,2,512,256]{3,2,0,1:T(8,128)(2,1)}, u32[]{:S(2)}) copy-start(bf16[4,2,512,256]{3,2,0,1:T(8,128)(2,1)} %copy.26) | copy-start | bytes 6291460
  157.8 4.7 %copy-start.5 = (bf16[2,512,2048]{2,1,0:T(8,128)(2,1)S(1)}, bf16[2,512,2048]{2,1,0:T(8,128)(2,1)}, u32[]{:S(2)}) copy-start(bf16[2,512,2048]{2,1,0:T(8,128)(2,1)} %all-gather.3.cloned.1.call-done) | copy-start | bytes 12582916
  207.4 5.8 %copy-start.3 = (f32[256,2]{0,1:T(2,128)S(1)}, f32[256,2]{0,1:T(2,128)}, u32[]{:S(2)}) copy-start(f32[256,2]{0,1:T(2,128)} %param.9) | copy-start | bytes 6148
  209.5 28.8 %all-to-all-start.4 = ((bf16[2,512,512]{2,0,1:T(2,128)(2,1)}), bf16[2,512,512]{2,0,1:T(2,128)(2,1)S(1)}, u32[]{:S(2)}, u32[]{:S(2)}) async-start(bf16[2,512,512]{2,0,1:T(2,128)(2,1)} %copy.32), calls=%async_computation.4 | async-start | bytes 2097152 | tf_op jit(solution)/shard_map/all_to_all | solution.py:59
Sparse Core Ops, SparseCore 0:
  53.5 35.8 all-gather.2
  164.8 24.1 all-gather.4
where the time goes:
time: 251 us; the launch traced here: 250 us
  waiting for transfers between devices  171 us (68%)
  starting transfers between devices  21.8 us (9%)
  local copies, waits for them, and re-layouts  17.5 us (7%)
  other arithmetic  15.5 us (6%)
  between operations  14.3 us (6%)
  matrix products  9.85 us (4%)
    all_to_all x1, waiting for transfers between devices, on_device(): lax.all_to_all(gate_local, 'fs', split_axis=0, concat_axis=1, tiled=True)  46.5 us
    all_to_all x1, waiting for transfers between devices, on_device(): lax.all_to_all(up_local, 'fs', split_axis=0, concat_axis=1, tiled=True)  42.6 us
    all_to_all x1, waiting for transfers between devices, on_device(): lax.all_to_all(down_local, 'fs', split_axis=0, concat_axis=1, tiled=True)  37.8 us
    all_to_all x1, waiting for transfers between devices, on_device(): lax.all_to_all(expert_out, 'fs', split_axis=1, concat_axis=0, tiled=True)  24.9 us
    all_to_all x1, waiting for transfers between devices, on_device(): lax.all_to_all(fill_slots(own_cols, targets, experts, capacity), 'fs', sp...  19.3 us
    convert_element_type x1, other arithmetic, on_device(): up_local = (up_master * row_gain).astype(jnp.bfloat16)  6.46 us
    all_to_all x1, starting transfers between devices, on_device(): lax.all_to_all(fill_slots(own_cols, targets, experts, capacity), 'fs', sp...  6.35 us
  transfers between devices with their start and end apart: 7, of which 5 were waited for; matrix products, arithmetic and copies ran while one was open for 10% of the time, Pallas kernels for 0%

commit v1 on v0

--- a/solution.py
+++ b/solution.py
@@ -39,13 +39,19 @@
     targets = slot_targets(route_ids, experts, capacity)
     col_width = normed.shape[1] // lax.axis_size("tp")
     own_cols = lax.dynamic_slice_in_dim(normed, lax.axis_index("tp") * col_width, col_width, 1)
-    part_rows = lax.all_to_all(
-        fill_slots(own_cols, targets, experts, capacity),
-        "fs",
-        split_axis=0,
-        concat_axis=1,
-        tiled=True,
-    )
+    value = fill_slots(own_cols, targets, experts, capacity)
+    ways, here = (lax.axis_size("fs"), lax.axis_index("fs"))
+    width = value.shape[0] // ways
+    lengths = list(value.shape)
+    lengths[0] = width
+    height = lengths[1]
+    lengths[1] = height * ways
+    part_rows = jnp.zeros(lengths, value.dtype)
+    for mask in range(ways):
+        part = lax.dynamic_slice_in_dim(value, (here ^ mask) * width, width, axis=0)
+        if mask:
+            part = lax.ppermute(part, "fs", [(d, d ^ mask) for d in range(ways)])
+        part_rows = lax.dynamic_update_slice_in_dim(part_rows, part, (here ^ mask) * height, axis=1)
     portion = lax.all_gather(part_rows, "tp", axis=2, tiled=True)
     gate_part = jnp.einsum("erd,edf->erf", portion, gate_serve, preferred_element_type=jnp.float32)
     up_part = jnp.einsum("erd,edf->erf", portion, up_serve, preferred_element_type=jnp.float32)

time: 251 us -> 241 us (0.960)
  waiting for transfers between devices: 171 us -> 158 us
    all_to_all x1 -> x0, waiting for transfers between devices: 19.3 us -> none  [on_device(): lax.all_to_all(fill_slots(own_cols, targets, experts, capacity), 'fs', sp...]
    ppermute x0 -> x3, waiting for transfers between devices: none -> 17.8 us  [on_device(): part = lax.ppermute(part, 'fs', [(d, d ^ mask) for d in range(ways)])]
    all_to_all x1, waiting for transfers between devices: 46.5 us -> 35.8 us  [on_device(): lax.all_to_all(gate_local, 'fs', split_axis=0, concat_axis=1, tiled=True)]
    all_to_all x1 -> x0, starting transfers between devices: 6.35 us -> none  [on_device(): lax.all_to_all(fill_slots(own_cols, targets, experts, capacity), 'fs', sp...]
    ppermute x0 -> x3, starting transfers between devices: none -> 5.64 us  [on_device(): part = lax.ppermute(part, 'fs', [(d, d ^ mask) for d in range(ways)])]
  transfers between devices with their start and end apart: 7 -> 9, of which waited for: 5 -> 5; matrix products, arithmetic and copies ran while one was open for 10% -> 10% of each run, Pallas kernels for 0% -> 0%
where the time goes in v1:
time: 241 us; the launch traced here: 240 us
  waiting for transfers between devices  158 us (66%)
  starting transfers between devices  22.6 us (9%)
  local copies, waits for them, and re-layouts  19.6 us (8%)
  other arithmetic  15.5 us (6%)
  between operations  14.3 us (6%)
  matrix products  9.86 us (4%)
    all_to_all x1, waiting for transfers between devices, on_device(): lax.all_to_all(up_local, 'fs', split_axis=0, concat_axis=1, tiled=True)  42.2 us
    all_to_all x1, waiting for transfers between devices, on_device(): lax.all_to_all(down_local, 'fs', split_axis=0, concat_axis=1, tiled=True)  37.8 us
    all_to_all x1, waiting for transfers between devices, on_device(): lax.all_to_all(gate_local, 'fs', split_axis=0, concat_axis=1, tiled=True)  35.8 us
    all_to_all x1, waiting for transfers between devices, on_device(): lax.all_to_all(expert_out, 'fs', split_axis=1, concat_axis=0, tiled=True)  24.9 us
    ppermute x3, waiting for transfers between devices, on_device(): part = lax.ppermute(part, 'fs', [(d, d ^ mask) for d in range(ways)])  17.8 us
    convert_element_type x1, other arithmetic, on_device(): up_local = (up_master * row_gain).astype(jnp.bfloat16)  6.46 us
    ppermute x3, starting transfers between devices, on_device(): part = lax.ppermute(part, 'fs', [(d, d ^ mask) for d in range(ways)])  5.64 us
    all_to_all x1, starting transfers between devices, on_device(): lax.all_to_all(gate_local, 'fs', split_axis=0, concat_axis=1, tiled=True)  5.09 us
  transfers between devices with their start and end apart: 9, of which 5 were waited for; matrix products, arithmetic and copies ran while one was open for 10% of the time, Pallas kernels for 0%

profile of v1, /device:TPU:0, one launch (start us, length us, event | category | flops | bytes accessed | tf_op | source)
XLA Modules:
  0.0 240.3 jit_solution(7443260357843464789)
XLA Ops:
  7.2 1.5 convert_element_type.43
  11.9 2.7 %scatter_custom_fusion = bf16[1024,512]{1,0:T(8,128)(2,1)S(1)} fusion(s32[512]{0:T(512)S(1)} %bitcast.44, bf16[512,512]{1,0:T(8,128)(2,1)S(1)} %reshape.101, bf16[]{:T(256)} %constant.16.clone.1), kind=kCustom, calls=%fused_computation.10 | custom fusion | bytes 1048578 | tf_op jit(solution)/shard_map/scatter | solution.py:19
  15.7 3.1 %collective-permute-start = (bf16[2,128,512]{2,1,0:T(8,128)(2,1)}, bf16[2,128,512]{2,1,0:T(8,128)(2,1)}, u32[]{:S(2)}, u32[]{:S(2)}) collective-permute-start(bf16[2,128,512]{2,1,0:T(8,128)(2,1)} %get-tuple-element.6), channel_id=1, source_target_pairs={{0,4},{4,0},{8,12},{12,8},{1,5},{5,1},{9,13},{13,9},{2,6},{6,2},{1... | collective-permute-start | bytes 786440 | tf_op jit(solution)/shard_map/ppermute | solution.py:53
  18.7 2.6 %collective-permute-start.1 = (bf16[2,128,512]{2,1,0:T(8,128)(2,1)}, bf16[2,128,512]{2,1,0:T(8,128)(2,1)}, u32[]{:S(2)}, u32[]{:S(2)}) collective-permute-start(bf16[2,128,512]{2,1,0:T(8,128)(2,1)} %get-tuple-element.5), channel_id=1, source_target_pairs={{0,8},{4,12},{8,0},{12,4},{1,9},{5,13},{9,1},{13,5},{2,10},{6,14},... | collective-permute-start | bytes 786440 | tf_op jit(solution)/shard_map/ppermute | solution.py:53
  21.3 6.5 %multiply_convert_fusion = (bf16[8,512,256]{2,1,0:T(8,128)(2,1)}, bf16[8,512,256]{2,1,0:T(8,128)(2,1)}) fusion(f32[8,512,256]{2,1,0:T(8,128)} %param.12, f32[512]{0:T(512)S(1)} %copy-done.5, f32[8,512,256]{2,1,0:T(8,128)} %param.11), kind=kLoop, calls=%fused_computation.2 | loop fusion | flops 4194304 | bytes 12584960 | tf_op jit(solution)/shard_map/convert_element_type | solution.py:26
  27.8 5.1 %all-to-all-start = ((bf16[8,512,256]{2,1,0:T(8,128)(2,1)}), bf16[8,512,256]{2,1,0:T(8,128)(2,1)S(1)}, u32[]{:S(2)}, u32[]{:S(2)}) async-start(bf16[8,512,256]{2,1,0:T(8,128)(2,1)} %get-tuple-element.9), calls=%async_computation | async-start | bytes 4194304 | tf_op jit(solution)/shard_map/all_to_all | solution.py:29
  33.9 17.8 %collective-permute-done.1 = bf16[2,128,512]{2,1,0:T(8,128)(2,1)} collective-permute-done((bf16[2,128,512]{2,1,0:T(8,128)(2,1)}, bf16[2,128,512]{2,1,0:T(8,128)(2,1)}, u32[]{:S(2)}, u32[]{:S(2)}) %collective-permute-start.1) | collective-permute-done | bytes 262176 | tf_op jit(solution)/shard_map/ppermute | solution.py:53
  53.7 35.8 %all-to-all-done = bf16[8,512,256]{2,1,0:T(8,128)(2,1)S(1)} async-done(((bf16[8,512,256]{2,1,0:T(8,128)(2,1)}), bf16[8,512,256]{2,1,0:T(8,128)(2,1)S(1)}, u32[]{:S(2)}, u32[]{:S(2)}) %all-to-all-start) | async-done | bytes 2097184 | tf_op jit(solution)/shard_map/all_to_all | solution.py:29
  89.5 4.5 %all-to-all-start.1 = ((bf16[8,512,256]{2,1,0:T(8,128)(2,1)}), bf16[8,512,256]{2,1,0:T(8,128)(2,1)}, u32[]{:S(2)}, u32[]{:S(2)}) async-start(bf16[8,512,256]{2,1,0:T(8,128)(2,1)} %get-tuple-element.8), calls=%async_computation.1 | async-start | bytes 4194304 | tf_op jit(solution)/shard_map/all_to_all | solution.py:30
  94.0 3.8 %convert_element_type.40 = bf16[8,256,512]{2,1,0:T(8,128)(2,1)} convert(f32[8,256,512]{2,1,0:T(8,128)} %param.13) | non-fusion elementwise | flops 1048576 | bytes 6291456 | tf_op jit(solution)/shard_map/convert_element_type | solution.py:27
  97.7 1.5 copy.24
  99.2 42.2 %all-to-all-done.1 = bf16[8,512,256]{2,1,0:T(8,128)(2,1)} async-done(((bf16[8,512,256]{2,1,0:T(8,128)(2,1)}), bf16[8,512,256]{2,1,0:T(8,128)(2,1)}, u32[]{:S(2)}, u32[]{:S(2)}) %all-to-all-start.1) | async-done | bytes 2097184 | tf_op jit(solution)/shard_map/all_to_all | solution.py:30
  141.4 3.6 %all-to-all-start.2 = ((bf16[8,256,512]{2,1,0:T(8,128)(2,1)}), bf16[8,256,512]{2,1,0:T(8,128)(2,1)S(1)}, u32[]{:S(2)}, u32[]{:S(2)}) async-start(bf16[8,256,512]{2,1,0:T(8,128)(2,1)} %convert_element_type.40), calls=%async_computation.2 | async-start | bytes 4194304 | tf_op jit(solution)/shard_map/all_to_all | solution.py:31
  145.1 3.0 %copy.25 = bf16[4,2,512,256]{3,2,0,1:T(8,128)(2,1)} copy(bf16[4,2,512,256]{3,2,1,0:T(8,128)(2,1)} %bitcast.3) | data formatting | bytes 4194304 | tf_op jit(solution)/shard_map/all_to_all | solution.py:30
  148.1 4.2 %fusion.6 = f32[2,512,256]{2,1,0:T(8,128)S(1)} fusion(bf16[2,512,2048]{2,1,0:T(8,128)(2,1)} %all-gather.3.cloned.1.call-done, bf16[2,2048,256]{2,1,0:T(8,128)(2,1)} %bitcast.38), kind=kOutput, calls=%fused_computation.30 | convolution fusion | flops 1073741824 | bytes 7340032 | tf_op jit(solution)/shard_map/erd,edf->erf/dot_general | solution.py:56
  152.8 2.1 multiply_convert_fusion.2
  155.0 37.8 %all-to-all-done.2 = bf16[8,256,512]{2,1,0:T(8,128)(2,1)S(1)} async-done(((bf16[8,256,512]{2,1,0:T(8,128)(2,1)}), bf16[8,256,512]{2,1,0:T(8,128)(2,1)S(1)}, u32[]{:S(2)}, u32[]{:S(2)}) %all-to-all-start.2) | async-done | bytes 2097184 | tf_op jit(solution)/shard_map/all_to_all | solution.py:31
  192.7 1.5 copy.26
  194.3 3.5 %convolution_convert_fusion = bf16[2,512,512]{2,1,0:T(8,128)(2,1)S(1)} fusion(bf16[2,512,1024]{2,1,0:T(8,128)(2,1)} %all-gather.5.cloned.1.call-done, bf16[2,1024,512]{2,1,0:T(8,128)(2,1)} %bitcast.42), kind=kOutput, calls=%fused_computation.5 | convolution fusion | flops 1074266112 | bytes 5242880 | tf_op jit(solution)/shard_map/erf,efd->erd/dot_general | solution.py:59
  197.8 2.1 copy.30
  199.8 3.7 %all-to-all-start.3 = ((bf16[2,512,512]{2,0,1:T(2,128)(2,1)}), bf16[2,512,512]{2,0,1:T(2,128)(2,1)S(1)}, u32[]{:S(2)}, u32[]{:S(2)}) async-start(bf16[2,512,512]{2,0,1:T(2,128)(2,1)} %copy.30), calls=%async_computation.3 | async-start | bytes 2097152 | tf_op jit(solution)/shard_map/all_to_all | solution.py:65
  203.7 24.9 %all-to-all-done.3 = bf16[2,512,512]{2,0,1:T(2,128)(2,1)S(1)} async-done(((bf16[2,512,512]{2,0,1:T(2,128)(2,1)}), bf16[2,512,512]{2,0,1:T(2,128)(2,1)S(1)}, u32[]{:S(2)}, u32[]{:S(2)}) %all-to-all-start.3) | async-done | bytes 1048608 | tf_op jit(solution)/shard_map/all_to_all | solution.py:65
  228.8 2.0 gather_fusion
  231.4 2.1 multiply_reduce_fusion.1
  (50 shorter events, 8.6 us)
Async XLA Ops:
  7.2 1.6 copy-start
  7.2 1.9 copy-start.3
  11.9 9.4 %copy-start.5 = (f32[512]{0:T(512)S(1)}, f32[512]{0:T(512)}, u32[]{:S(2)}) copy-start(f32[512]{0:T(512)} %param.10) | copy-start | bytes 6148
  15.7 17.2 %collective-permute-start = (bf16[2,128,512]{2,1,0:T(8,128)(2,1)}, bf16[2,128,512]{2,1,0:T(8,128)(2,1)}, u32[]{:S(2)}, u32[]{:S(2)}) collective-permute-start(bf16[2,128,512]{2,1,0:T(8,128)(2,1)} %get-tuple-element.6), channel_id=1, source_target_pairs={{0,4},{4,0},{8,12},{12,8},{1,5},{5,1},{9,13},{13,9},{2,6},{6,2},{1... | collective-permute-start | bytes 786440 | tf_op jit(solution)/shard_map/ppermute | solution.py:53
  18.7 32.9 %collective-permute-start.1 = (bf16[2,128,512]{2,1,0:T(8,128)(2,1)}, bf16[2,128,512]{2,1,0:T(8,128)(2,1)}, u32[]{:S(2)}, u32[]{:S(2)}) collective-permute-start(bf16[2,128,512]{2,1,0:T(8,128)(2,1)} %get-tuple-element.5), channel_id=1, source_target_pairs={{0,8},{4,12},{8,0},{12,4},{1,9},{5,13},{9,1},{13,5},{2,10},{6,14},... | collective-permute-start | bytes 786440 | tf_op jit(solution)/shard_map/ppermute | solution.py:53
  21.3 31.3 %collective-permute-start.2 = (bf16[2,128,512]{2,1,0:T(8,128)(2,1)}, bf16[2,128,512]{2,1,0:T(8,128)(2,1)S(1)}, u32[]{:S(2)}, u32[]{:S(2)}) collective-permute-start(bf16[2,128,512]{2,1,0:T(8,128)(2,1)} %get-tuple-element.4), channel_id=1, source_target_pairs={{0,12},{4,8},{8,4},{12,0},{1,13},{5,9},{9,5},{13,1},{2,14},{6,10},... | collective-permute-start | bytes 786440 | tf_op jit(solution)/shard_map/ppermute | solution.py:53
  27.8 61.7 %all-to-all-start = ((bf16[8,512,256]{2,1,0:T(8,128)(2,1)}), bf16[8,512,256]{2,1,0:T(8,128)(2,1)S(1)}, u32[]{:S(2)}, u32[]{:S(2)}) async-start(bf16[8,512,256]{2,1,0:T(8,128)(2,1)} %get-tuple-element.9), calls=%async_computation | async-start | bytes 4194304 | tf_op jit(solution)/shard_map/all_to_all | solution.py:29
  32.9 115.2 %all-gather.3.cloned.1.call-start = ((), (), s32[]{:S(2)}) async-start(), calls=%async_computation.4 | async-start | bytes 5242880 | tf_op jit(solution)/shard_map/all_gather | solution.py:55
  52.6 1.1 copy-start.1
  89.5 51.9 %all-to-all-start.1 = ((bf16[8,512,256]{2,1,0:T(8,128)(2,1)}), bf16[8,512,256]{2,1,0:T(8,128)(2,1)}, u32[]{:S(2)}, u32[]{:S(2)}) async-start(bf16[8,512,256]{2,1,0:T(8,128)(2,1)} %get-tuple-element.8), calls=%async_computation.1 | async-start | bytes 4194304 | tf_op jit(solution)/shard_map/all_to_all | solution.py:30
  141.4 51.3 %all-to-all-start.2 = ((bf16[8,256,512]{2,1,0:T(8,128)(2,1)}), bf16[8,256,512]{2,1,0:T(8,128)(2,1)S(1)}, u32[]{:S(2)}, u32[]{:S(2)}) async-start(bf16[8,256,512]{2,1,0:T(8,128)(2,1)} %convert_element_type.40), calls=%async_computation.2 | async-start | bytes 4194304 | tf_op jit(solution)/shard_map/all_to_all | solution.py:31
  145.0 49.3 %all-gather.5.cloned.1.call-start = ((), (), s32[]{:S(2)}) async-start(), calls=%async_computation.5 | async-start | bytes 2621440 | tf_op jit(solution)/shard_map/all_gather | solution.py:61
  148.1 4.3 %copy-start.2 = (bf16[4,2,512,256]{3,2,0,1:T(8,128)(2,1)S(1)}, bf16[4,2,512,256]{3,2,0,1:T(8,128)(2,1)}, u32[]{:S(2)}) copy-start(bf16[4,2,512,256]{3,2,0,1:T(8,128)(2,1)} %copy.25) | copy-start | bytes 6291460
  148.1 4.7 %copy-start.6 = (bf16[2,512,2048]{2,1,0:T(8,128)(2,1)S(1)}, bf16[2,512,2048]{2,1,0:T(8,128)(2,1)}, u32[]{:S(2)}) copy-start(bf16[2,512,2048]{2,1,0:T(8,128)(2,1)} %all-gather.3.cloned.1.call-done) | copy-start | bytes 12582916
  197.8 5.8 %copy-start.4 = (f32[256,2]{0,1:T(2,128)S(1)}, f32[256,2]{0,1:T(2,128)}, u32[]{:S(2)}) copy-start(f32[256,2]{0,1:T(2,128)} %param.9) | copy-start | bytes 6148
  199.8 28.8 %all-to-all-start.3 = ((bf16[2,512,512]{2,0,1:T(2,128)(2,1)}), bf16[2,512,512]{2,0,1:T(2,128)(2,1)S(1)}, u32[]{:S(2)}, u32[]{:S(2)}) async-start(bf16[2,512,512]{2,0,1:T(2,128)(2,1)} %copy.30), calls=%async_computation.3 | async-start | bytes 2097152 | tf_op jit(solution)/shard_map/all_to_all | solution.py:65
Sparse Core Ops, SparseCore 0:
  53.8 37.1 all-gather.2
  155.1 24.1 all-gather.4
